TPU v7x, 32 devices: a whole 2x2x4 slice. The times are simulated.
32 devices in a mesh: ep: 8 (over z, y), tp: 4 (over x, core).
Axes of the slice: x: 2, y: 2, z: 4, core: 2. Of those that a mesh axis runs over, the one named last changes fastest.
Arguments:
- tokens: bfloat16 [256, 2048], P('ep'), may hold values from -6 to 6
- gain_mix: bfloat16 [2048], replicated, may hold values from 0.099609375 to 1.8984375
- gain_ffn: bfloat16 [2048], replicated, may hold values from 0.099609375 to 1.8984375
- w_query: bfloat16 [2048, 1024], P('ep', 'tp'), may hold values from -0.125 to 0.125
- w_key: bfloat16 [2048, 1024], P('ep', 'tp'), may hold values from -0.125 to 0.125
- w_value: bfloat16 [2048, 1024], P('ep', 'tp'), may hold values from -0.125 to 0.125
- w_outgate: bfloat16 [2048, 1024], P('ep', 'tp'), may hold values from -0.125 to 0.125
- w_ingate: bfloat16 [2048, 8], replicated, may hold values from -0.125 to 0.125
- w_forget: bfloat16 [2048, 8], replicated, may hold values from -0.125 to 0.125
- bias_in: float32 [8], replicated, may hold values from -2 to 2
- bias_forget: float32 [8], replicated, may hold values from -1 to 3
- w_proj: bfloat16 [1024, 2048], P('tp'), may hold values from -0.1875 to 0.1875
- matrix_state: float32 [256, 8, 128, 128], P('ep', 'tp'), may hold values from -0.6 to 0.6
- normal_state: float32 [256, 8, 128], P('ep', 'tp'), may hold values from -0.6 to 0.6
- stab_state: float32 [256, 8], P('ep', 'tp'), may hold values from -1 to 1
- route_ids: int32 [256, 2], P('ep'), may hold values from 0 to 3, all different within a row; in each aligned block of 32 rows (0 to 31, 32 to 63, ...) at most 32 rows name the same one
- route_weights: float32 [256, 2], P('ep'), may hold values from 0.1 to 1
- w_exp_gate: bfloat16 [8, 2048, 1536], P('ep', None, 'tp'), may hold values from -0.125 to 0.125
- w_exp_up: bfloat16 [8, 2048, 1536], P('ep', None, 'tp'), may hold values from -0.125 to 0.125
- w_exp_down: bfloat16 [8, 1536, 2048], P('ep', 'tp'), may hold values from -0.109375 to 0.109375
Outputs:
- mixed_out: bfloat16 [256, 2048], P('ep', 'tp')
- matrix_out: float32 [256, 8, 128, 128], P('ep', 'tp')
- normal_out: float32 [256, 8, 128], P('ep', 'tp')
- stab_out: float32 [256, 8], P('ep', 'tp')
Inputs may be any that keep to these rules, and one draw needn't show every extreme that they name: `route_ids`: each row names 2 different experts; among the rows of one index of ep no expert is named by more than 32 rows, and in every draw some expert is named by exactly 32 of them.
All inputs are finite; a program needn't handle non-finite values.
Results may differ from a plain program's by a relative error of at most 0.015.
Values may be sent and summed in bfloat16 or wider, within the bound.
No kernel may reach another device: no remote copies, remote signals or barrier semaphores. Data moves between devices by JAX's collectives and lax.ppermute only.
A program may use at most 64 MiB of HBM per device.

v0:
```python
import jax
import jax.numpy as jnp
from jax import lax
from jax.sharding import PartitionSpec as P

norm_epsilon = 1e-06


def rms_scale(row_block, gain):
    wide = row_block.astype(jnp.float32)
    factor = lax.rsqrt(jnp.mean(wide * wide, axis=-1, keepdims=True) + norm_epsilon)
    return (wide * factor * gain.astype(jnp.float32)).astype(jnp.bfloat16)


def memory_step(
    query,
    key_rows,
    value_rows,
    gate_rows,
    in_pre,
    forget_pre,
    matrix_state,
    normal_state,
    stab_state,
):
    log_forget = jax.nn.log_sigmoid(forget_pre)
    stab_new = jnp.maximum(log_forget + stab_state, in_pre)
    carry = jnp.exp(log_forget + stab_state - stab_new)
    inflow = jnp.exp(in_pre - stab_new)
    scaled_keys = key_rows.astype(jnp.float32) * query.shape[-1] ** (-0.5)
    value_wide = value_rows.astype(jnp.float32)
    matrix_new = (
        carry[..., None, None] * matrix_state
        + inflow[..., None, None] * scaled_keys[..., :, None] * value_wide[..., None, :]
    )
    normal_new = carry[..., None] * normal_state + inflow[..., None] * scaled_keys
    query_wide = query.astype(jnp.float32)
    numer = jnp.einsum("shd,shde->she", query_wide, matrix_new, precision=lax.Precision.HIGHEST)
    denom = jnp.maximum(jnp.abs(jnp.sum(query_wide * normal_new, axis=-1)), 1.0)
    hidden = numer / denom[..., None] * jax.nn.sigmoid(gate_rows.astype(jnp.float32))
    return (hidden, matrix_new, normal_new, stab_new)


def dispatch_table(route_ids, experts, capacity):
    flat_ids = route_ids.reshape(-1)
    expert_hot = (flat_ids[:, None] == jnp.arange(experts, dtype=jnp.int32)[None, :]).astype(
        jnp.int32
    )
    slot_rank = jnp.sum((jnp.cumsum(expert_hot, axis=0) - 1) * expert_hot, axis=1)
    slot_hot = (slot_rank[:, None] == jnp.arange(capacity, dtype=jnp.int32)[None, :]).astype(
        jnp.float32
    )
    table = expert_hot.astype(jnp.float32)[:, :, None] * slot_hot[:, None, :]
    return table.reshape(flat_ids.shape[0], experts * capacity)


def send_rows(table, row_block, top_count, experts, capacity):
    repeated = jnp.repeat(row_block, top_count, axis=0)
    packed = jnp.einsum(
        "as,aw->sw", table.astype(jnp.bfloat16), repeated, preferred_element_type=jnp.float32
    ).astype(jnp.bfloat16)
    row_width = row_block.shape[1]
    doubled = jnp.broadcast_to(
        packed.reshape(experts, 1, capacity, row_width), (experts, 2, capacity, row_width)
    )
    return doubled.reshape(experts * 2 * capacity, row_width)


def body(
    tokens,
    gain_mix,
    gain_ffn,
    w_query,
    w_key,
    w_value,
    w_outgate,
    w_ingate,
    w_forget,
    bias_in,
    bias_forget,
    w_proj,
    matrix_state,
    normal_state,
    stab_state,
    route_ids,
    route_weights,
    w_exp_gate,
    w_exp_up,
    w_exp_down,
):
    ep_count = lax.axis_size("ep")
    tp_count = lax.axis_size("tp")
    tp_index = lax.axis_index("tp")
    seq_dev = tokens.shape[0]
    model_width = tokens.shape[1]
    heads_dev = matrix_state.shape[1]
    head_dim = matrix_state.shape[2]
    head_cols = w_query.shape[1]
    top_count = route_ids.shape[1]
    experts = ep_count // 2
    capacity = min(seq_dev, max(2, 2 * seq_dev * top_count // experts))
    col_width = model_width // tp_count
    normed = rms_scale(tokens, gain_mix)
    foreign = lax.all_to_all(normed, "ep", split_axis=1, concat_axis=0, tiled=True)
    summed = lax.psum_scatter(
        jnp.concatenate(
            [
                jnp.dot(foreign, weight, preferred_element_type=jnp.float32)
                for weight in (w_query, w_key, w_value, w_outgate)
            ],
            axis=1,
        ),
        "ep",
        scatter_dimension=0,
        tiled=True,
    )
    partials = [summed[:, offset * head_cols : (offset + 1) * head_cols] for offset in range(4)]
    query, key_rows, value_rows, gate_rows = [
        partial_value.astype(jnp.bfloat16).reshape(seq_dev, heads_dev, head_dim)
        for partial_value in partials
    ]
    head_first = tp_index * heads_dev
    in_pre = lax.dynamic_slice_in_dim(
        jnp.dot(normed, w_ingate, preferred_element_type=jnp.float32) + bias_in,
        head_first,
        heads_dev,
        1,
    )
    forget_pre = lax.dynamic_slice_in_dim(
        jnp.dot(normed, w_forget, preferred_element_type=jnp.float32) + bias_forget,
        head_first,
        heads_dev,
        1,
    )
    hidden, matrix_new, normal_new, stab_new = memory_step(
        query,
        key_rows,
        value_rows,
        gate_rows,
        in_pre,
        forget_pre,
        matrix_state,
        normal_state,
        stab_state,
    )
    cell = hidden.reshape(seq_dev, head_cols).astype(jnp.bfloat16)
    partial_out = jnp.dot(cell, w_proj, preferred_element_type=jnp.float32)
    table = dispatch_table(route_ids, experts, capacity)
    gate_local = w_exp_gate[0]
    up_local = w_exp_up[0]
    attended = lax.psum(partial_out.astype(jnp.bfloat16), "tp").astype(jnp.float32)
    resid = (tokens.astype(jnp.float32) + attended).astype(jnp.bfloat16)
    normed_ffn = rms_scale(resid, gain_ffn)
    own_resid = lax.dynamic_slice_in_dim(resid, tp_index * col_width, col_width, 1)
    outgoing = send_rows(table, normed_ffn, top_count, experts, capacity)
    received = lax.all_to_all(outgoing, "ep", split_axis=0, concat_axis=0, tiled=True)
    gate_sum = jnp.dot(received, gate_local, preferred_element_type=jnp.float32)
    up_sum = jnp.dot(received, up_local, preferred_element_type=jnp.float32)
    inner = (jax.nn.silu(gate_sum) * up_sum).astype(jnp.bfloat16)
    expert_terms = jnp.dot(inner, w_exp_down[0], preferred_element_type=jnp.float32)
    half_share = lax.psum_scatter(
        expert_terms.astype(jnp.bfloat16), "tp", scatter_dimension=1, tiled=True
    )
    returned = lax.all_to_all(half_share, "ep", split_axis=0, concat_axis=0, tiled=True)
    halves_summed = jnp.sum(
        returned.astype(jnp.float32).reshape(experts, 2, capacity, col_width), axis=1
    ).reshape(experts * capacity, col_width)
    weights = route_weights / jnp.sum(route_weights, axis=-1, keepdims=True)
    combine = jnp.sum(
        (table * weights.reshape(-1)[:, None]).reshape(seq_dev, top_count, experts * capacity),
        axis=1,
    )
    routed = jnp.dot(combine, halves_summed, precision=lax.Precision.HIGHEST)
    mixed_out = (own_resid.astype(jnp.float32) + routed).astype(jnp.bfloat16)
    return (mixed_out, matrix_new, normal_new, stab_new)


def solution(mesh):
    placed = (
        P("ep", None),
        P(),
        P(),
        P("ep", "tp"),
        P("ep", "tp"),
        P("ep", "tp"),
        P("ep", "tp"),
        P(),
        P(),
        P(),
        P(),
        P("tp", None),
        P("ep", "tp", None, None),
        P("ep", "tp", None),
        P("ep", "tp"),
        P("ep", None),
        P("ep", None),
        P("ep", None, "tp"),
        P("ep", None, "tp"),
        P("ep", "tp", None),
    )
    return jax.shard_map(
        body,
        mesh=mesh,
        in_specs=placed,
        out_specs=(P("ep", "tp"), P("ep", "tp", None, None), P("ep", "tp", None), P("ep", "tp")),
        check_vma=False,
    )
```

profile of v0, /device:TPU:0, one launch (start us, length us, event | category | flops | bytes accessed | tf_op | source)
XLA Modules:
  0.0 213.6 jit_solution(9406941949861868896)
XLA Ops:
  7.2 0.0 copy-start
  7.2 0.0 reduce-scatter.7.cloned.1.call-start
  7.2 1.2 fusion.22
  8.4 0.7 convert_element_type.121
  9.1 1.0 fusion.24
  10.1 14.5 %all_to_all.40 = bf16[32,8,256]{2,0,1:T(8,128)(2,1)S(1)} all-to-all(bf16[32,8,256]{2,0,1:T(8,128)(2,1)S(1)} %bitcast.72), channel_id=1, replica_groups=mesh['ep'=8,'tp'=4] {'ep'}, dimensions={1} | all-to-all | bytes 262144 | tf_op jit(solution)/shard_map/all_to_all | solution.py:104
  24.6 1.1 fusion.41
  25.7 1.1 fusion.40
  26.9 0.2 fusion.39
  27.1 0.2 fusion.38
  27.3 0.1 pad_maximum_fusion
  27.4 0.0 copy-start.10
  27.4 0.0 copy-start.14
  27.5 0.0 copy-start.13
  27.5 1.3 copy.72
  28.8 0.0 reduce-scatter.7.cloned.1.call-update
  28.8 0.0 all-reduce.2.cloned.1.call-start
  28.9 0.1 copy.63
  29.0 0.1 eq.36
  29.1 0.1 fusion.29
  29.2 0.1 copy.64
  29.2 0.1 reduce_window_sum.11
  29.4 0.1 convolution_add_fusion.1
  29.5 0.0 copy-done.13
  29.5 0.1 convolution_add_fusion.2
  29.7 0.0 copy-done.11
  29.7 0.0 copy-start.9
  29.7 0.1 copy.56
  29.8 0.1 copy.57
  29.9 0.2 select_reduce_fusion
  30.1 61.5 %reduce-scatter.7.cloned.1.call-done = f32[32,1024]{1,0:T(8,128)} async-done(((f32[256,1024]{1,0:T(8,128)}), f32[32,1024]{1,0:T(8,128)}) %reduce-scatter.7.cloned.1.call-update) | async-done | bytes 131088
  91.6 1.1 copy.73
  92.7 0.1 copy.60
  92.8 0.1 copy.74
  92.9 0.1 copy.58
  93.0 0.1 copy.59
  93.1 0.8 multiply_reduce_fusion.2
  93.9 0.1 copy.62
  94.0 6.0 %multiply_reduce_fusion = (f32[32,2,128]{2,1,0:T(2,128)S(1)}, f32[32,2,128,128]{3,2,1,0:T(8,128)}) fusion(f32[32,2,128]{2,1,0:T(2,128)S(1)} %copy.74, f32[32,2,128]{2,1,0:T(2,128)S(1)} %copy.59, f32[32,2,128]{2,1,0:T(2,128)S(1)} %get-tuple-element.8, f32[32,2,128,128]{3,2,1,0:T(8,128)} %param.32, f32[32,2]{1,0:T(8,128)S(1)} %copy.56), kind=kLoop, calls=%fused_computation | loop fusion | flops 5234688 | bytes 8519936
  99.9 0.0 copy-start.7
  100.0 0.0 copy-start.2
  100.0 0.1 copy.71
  100.1 1.0 convolution_convert_fusion.2
  101.1 0.0 all-reduce.2.cloned.1.call-update
  101.1 0.0 reduce-scatter.5.cloned.1.call-start
  101.2 30.9 %all-reduce.2.cloned.1.call-done = bf16[32,2048]{1,0:T(8,128)(2,1)} async-done(((bf16[32,2048]{1,0:T(8,128)(2,1)}), bf16[32,2048]{1,0:T(8,128)(2,1)}) %all-reduce.2.cloned.1.call-update) | async-done | bytes 131088 | tf_op jit(solution)/shard_map/psum | solution.py:151
  132.1 1.1 fusion.19
  133.1 0.1 fusion.21
  133.3 0.1 broadcast_in_dim.6
  133.4 0.1 reshape.157
  133.5 0.3 convolution_convert_fusion.1
  133.8 0.1 broadcast_in_dim.8
  133.9 30.2 %all_to_all.41 = bf16[8,32,2048]{2,1,0:T(8,128)(2,1)S(1)} all-to-all(bf16[8,32,2048]{2,1,0:T(8,128)(2,1)S(1)} %bitcast.61), channel_id=1, replica_groups=mesh['ep'=8,'tp'=4] {'ep'}, dimensions={0} | all-to-all | bytes 2097152 | tf_op jit(solution)/shard_map/all_to_all | solution.py:156
  164.1 0.7 fusion.3
  164.9 3.7 %convolution_convert_fusion = bf16[256,2048]{1,0:T(8,128)(2,1)} fusion(bf16[1,384,2048]{2,1,0:T(8,128)(2,1)S(1)} %copy-done, bf16[256,2048]{1,0:T(8,128)(2,1)S(1)} %bitcast.60, bf16[1,2048,384]{2,1,0:T(8,128)(2,1)} %param.38, f32[256,384]{1,0:T(8,128)S(1)} %fusion.3), kind=kOutput, calls=%fused_computation.2 | convolution fusion | flops 806420480 | bytes 5636096 | tf_op jit(solution)/shard_map/dot_general | solution.py:160
  168.6 0.0 reduce-scatter.5.cloned.1.call-update
  168.6 23.2 %reduce-scatter.5.cloned.1.call-done = bf16[256,512]{1,0:T(8,128)(2,1)} async-done(((bf16[256,2048]{1,0:T(8,128)(2,1)}), bf16[256,512]{1,0:T(8,128)(2,1)}) %reduce-scatter.5.cloned.1.call-update) | async-done | bytes 262160 | tf_op jit(solution)/shard_map/reduce_scatter | solution.py:161
  191.8 5.5 %all-to-all-start.2 = ((bf16[8,32,512]{2,1,0:T(8,128)(2,1)}), bf16[8,32,512]{2,1,0:T(8,128)(2,1)S(1)}, u32[]{:S(2)}, u32[]{:S(2)}) async-start(bf16[8,32,512]{2,1,0:T(8,128)(2,1)} %bitcast.74), calls=%async_computation.3 | async-start | bytes 524288 | tf_op jit(solution)/shard_map/all_to_all | solution.py:164
  197.4 0.1 copy.66
  197.5 0.1 copy.65
  197.6 0.1 mul.171
  197.7 0.1 multiply_reduce_fusion.1
  197.8 8.3 %all-to-all-done.2 = bf16[8,32,512]{2,1,0:T(8,128)(2,1)S(1)} async-done(((bf16[8,32,512]{2,1,0:T(8,128)(2,1)}), bf16[8,32,512]{2,1,0:T(8,128)(2,1)S(1)}, u32[]{:S(2)}, u32[]{:S(2)}) %all-to-all-start.2) | async-done | bytes 262176 | tf_op jit(solution)/shard_map/all_to_all | solution.py:164
  206.2 0.9 fusion.13
  (38 shorter events, 0.3 us)
Async XLA Ops:
  7.2 157.7 %copy-start = (bf16[1,384,2048]{2,1,0:T(8,128)(2,1)S(1)}, bf16[1,384,2048]{2,1,0:T(8,128)(2,1)}, u32[]{:S(2)}) copy-start(bf16[1,384,2048]{2,1,0:T(8,128)(2,1)} %param.39) | copy-start | bytes 4718596
  7.2 19.7 %copy-start.4 = (bf16[256,256]{1,0:T(8,128)(2,1)S(1)}, bf16[256,256]{1,0:T(8,128)(2,1)}, u32[]{:S(2)}) copy-start(bf16[256,256]{1,0:T(8,128)(2,1)} %param.24) | copy-start | bytes 393220
  7.2 19.9 %copy-start.5 = (bf16[256,256]{1,0:T(8,128)(2,1)S(1)}, bf16[256,256]{1,0:T(8,128)(2,1)}, u32[]{:S(2)}) copy-start(bf16[256,256]{1,0:T(8,128)(2,1)} %param.23) | copy-start | bytes 393220
  7.2 84.4 %reduce-scatter.7.cloned.1.call-start = ((), (), s32[]{:S(2)}) async-start(), calls=%async_computation.7 | async-start | bytes 1179648
  27.4 1.5 copy-start.10
  27.4 1.9 copy-start.12
  27.4 1.9 copy-start.14
  27.5 2.0 copy-start.13
  27.5 2.0 copy-start.15
  27.5 2.2 %copy-start.11 = (f32[32,2]{0,1:T(2,128)S(1)}, f32[32,2]{0,1:T(2,128)}, u32[]{:S(2)}) copy-start(f32[32,2]{0,1:T(2,128)} %param.34) | copy-start | bytes 772
  28.8 64.3 %copy-start.6 = (f32[32,2,128]{2,1,0:T(2,128)S(1)}, f32[32,2,128]{2,1,0:T(2,128)}, u32[]{:S(2)}) copy-start(f32[32,2,128]{2,1,0:T(2,128)} %param.33) | copy-start | bytes 98308
  28.8 103.2 %all-reduce.2.cloned.1.call-start = ((), (), s32[]{:S(2)}) async-start(), calls=%async_computation.5 | async-start | bytes 262144 | tf_op jit(solution)/shard_map/psum | solution.py:151
  29.7 70.2 %copy-start.9 = (f32[32,2]{0,1:T(2,128)}, f32[32,2]{0,1:T(2,128)S(1)}, u32[]{:S(2)}) copy-start(f32[32,2]{0,1:T(2,128)S(1)} %get-tuple-element.12) | copy-start | bytes 772
  94.0 6.1 %copy-start.3 = (bf16[256,2048]{1,0:T(8,128)(2,1)S(1)}, bf16[256,2048]{1,0:T(8,128)(2,1)}, u32[]{:S(2)}) copy-start(bf16[256,2048]{1,0:T(8,128)(2,1)} %param.31) | copy-start | bytes 3145732
  99.9 1.2 copy-start.7
  100.0 32.1 %copy-start.2 = (bf16[32,2048]{1,0:T(8,128)(2,1)S(1)}, bf16[32,2048]{1,0:T(8,128)(2,1)}, u32[]{:S(2)}) copy-start(bf16[32,2048]{1,0:T(8,128)(2,1)} %param.20) | copy-start | bytes 393220
  101.1 90.7 %reduce-scatter.5.cloned.1.call-start = ((), (), s32[]{:S(2)}) async-start(), calls=%async_computation.6 | async-start | bytes 1310720 | tf_op jit(solution)/shard_map/reduce_scatter | solution.py:161
  133.8 30.3 %copy-start.1 = (bf16[1,2048,384]{2,1,0:T(8,128)(2,1)S(1)}, bf16[1,2048,384]{2,1,0:T(8,128)(2,1)}, u32[]{:S(2)}) copy-start(bf16[1,2048,384]{2,1,0:T(8,128)(2,1)} %param.37) | copy-start | bytes 4718596
  168.6 28.7 %copy-start.8 = (f32[32,2]{0,1:T(2,128)S(1)}, f32[32,2]{0,1:T(2,128)}, u32[]{:S(2)}) copy-start(f32[32,2]{0,1:T(2,128)} %param.36) | copy-start | bytes 772
  191.8 14.3 %all-to-all-start.2 = ((bf16[8,32,512]{2,1,0:T(8,128)(2,1)}), bf16[8,32,512]{2,1,0:T(8,128)(2,1)S(1)}, u32[]{:S(2)}, u32[]{:S(2)}) async-start(bf16[8,32,512]{2,1,0:T(8,128)(2,1)} %bitcast.74), calls=%async_computation.3 | async-start | bytes 524288 | tf_op jit(solution)/shard_map/all_to_all | solution.py:164
Sparse Core Ops, SparseCore 0:
  29.0 62.5 reduce-scatter.6
  101.2 30.8 all-reduce.1
  168.8 23.0 reduce-scatter.4
where the time goes:
time: 214 us
  waiting for transfers between devices  124 us (58%)
  blocking collectives  44.6 us (21%)
  between operations  14.2 us (7%)
  other arithmetic  11.5 us (5%)
  matrix products  9.5 us (4%)
  starting transfers between devices  5.62 us (3%)
  local copies, waits for them, and re-layouts  4.18 us (2%)
    unnamed x4, waiting for transfers between devices  61.5 us
    psum x1, waiting for transfers between devices, body(): lax.psum(partial_out.astype(jnp.bfloat16), 'tp').astype(jnp.float32)  30.9 us
    all_to_all x1, blocking collectives, body(): lax.all_to_all(outgoing, 'ep', split_axis=0, concat_axis=0, tiled=True)  30.2 us
    reduce_scatter x1, waiting for transfers between devices, body(): lax.psum_scatter(expert_terms.astype(jnp.bfloat16), 'tp', scatter_dimensi...  23.2 us
    all_to_all x1, blocking collectives, body(): lax.all_to_all(normed, 'ep', split_axis=1, concat_axis=0, tiled=True)  14.5 us
    all_to_all x1, waiting for transfers between devices, body(): lax.all_to_all(half_share, 'ep', split_axis=0, concat_axis=0, tiled=True)  8.28 us
    unnamed x1, other arithmetic  5.95 us
    all_to_all x1, starting transfers between devices, body(): lax.all_to_all(half_share, 'ep', split_axis=0, concat_axis=0, tiled=True)  5.5 us
  transfers between devices with their start and end apart: 4, of which 4 were waited for; matrix products, arithmetic and copies ran while one was open for 1% of the time, Pallas kernels for 0%

commit v1 on v0

--- a/solution.py
+++ b/solution.py
@@ -148,7 +148,9 @@
     table = dispatch_table(route_ids, experts, capacity)
     gate_local = w_exp_gate[0]
     up_local = w_exp_up[0]
-    attended = lax.psum(partial_out.astype(jnp.bfloat16), "tp").astype(jnp.float32)
+    attended = jnp.sum(lax.all_gather(partial_out.astype(jnp.bfloat16), "tp"), axis=0).astype(
+        jnp.float32
+    )
     resid = (tokens.astype(jnp.float32) + attended).astype(jnp.bfloat16)
     normed_ffn = rms_scale(resid, gain_ffn)
     own_resid = lax.dynamic_slice_in_dim(resid, tp_index * col_width, col_width, 1)

time: 214 us -> 189 us (0.88)
  waiting for transfers between devices: 124 us -> 93.1 us
  blocking collectives: 44.6 us -> 51.4 us
    psum x1 -> x0, waiting for transfers between devices: 30.9 us -> none  [body(): lax.psum(partial_out.astype(jnp.bfloat16), 'tp').astype(jnp.float32)]
    all_gather x0 -> x1, blocking collectives: none -> 7.15 us  [body(): lax.all_gather(partial_out.astype(jnp.bfloat16), 'tp')]
    unnamed x4 -> x3, waiting for transfers between devices: 61.5 us -> 61.5 us
  transfers between devices with their start and end apart: 4 -> 3, of which waited for: 4 -> 3; matrix products, arithmetic and copies ran while one was open for 1% -> 1% of each run, Pallas kernels for 0% -> 0%
where the time goes in v1:
time: 189 us; the launch traced here: 188 us
  waiting for transfers between devices  93.1 us (49%)
  blocking collectives  51.4 us (27%)
  between operations  14.5 us (8%)
  other arithmetic  10.7 us (6%)
  matrix products  8.88 us (5%)
  starting transfers between devices  5.62 us (3%)
  local copies, waits for them, and re-layouts  4.18 us (2%)
    unnamed x3, waiting for transfers between devices  61.5 us
    all_to_all x1, blocking collectives, body(): lax.all_to_all(outgoing, 'ep', split_axis=0, concat_axis=0, tiled=True)  29.8 us
    reduce_scatter x1, waiting for transfers between devices, body(): lax.psum_scatter(expert_terms.astype(jnp.bfloat16), 'tp', scatter_dimensi...  23.3 us
    all_to_all x1, blocking collectives, body(): lax.all_to_all(normed, 'ep', split_axis=1, concat_axis=0, tiled=True)  14.5 us
    all_to_all x1, waiting for transfers between devices, body(): lax.all_to_all(half_share, 'ep', split_axis=0, concat_axis=0, tiled=True)  8.24 us
    all_gather x1, blocking collectives, body(): lax.all_gather(partial_out.astype(jnp.bfloat16), 'tp')  7.15 us
    unnamed x1, other arithmetic  5.95 us
    all_to_all x1, starting transfers between devices, body(): lax.all_to_all(half_share, 'ep', split_axis=0, concat_axis=0, tiled=True)  5.54 us
  transfers between devices with their start and end apart: 3, of which 3 were waited for; matrix products, arithmetic and copies ran while one was open for 1% of the time, Pallas kernels for 0%

profile of v1, /device:TPU:0, one launch (start us, length us, event | category | flops | bytes accessed | tf_op | source)
XLA Modules:
  0.0 188.3 jit_solution(18349755467467145281)
XLA Ops:
  7.2 0.0 copy-start
  7.2 0.0 reduce-scatter.7.cloned.1.call-start
  7.2 1.2 fusion.22
  8.4 0.7 convert_element_type.123
  9.1 1.0 fusion.24
  10.1 14.5 %all_to_all.40 = bf16[32,8,256]{2,0,1:T(8,128)(2,1)S(1)} all-to-all(bf16[32,8,256]{2,0,1:T(8,128)(2,1)S(1)} %bitcast.74), channel_id=1, replica_groups=mesh['ep'=8,'tp'=4] {'ep'}, dimensions={1} | all-to-all | bytes 262144 | tf_op jit(solution)/shard_map/all_to_all | solution.py:104
  24.6 1.1 fusion.41
  25.7 1.1 fusion.40
  26.9 0.2 fusion.39
  27.1 0.2 fusion.38
  27.4 0.1 pad_maximum_fusion
  27.4 0.0 copy-start.7
  27.4 0.0 copy-start.10
  27.5 0.0 copy-start.12
  27.5 0.0 copy-start.14
  27.5 0.0 copy-start.11
  27.5 1.3 copy.72
  28.8 0.0 reduce-scatter.7.cloned.1.call-update
  28.8 0.0 reduce-scatter.5.cloned.1.call-start
  28.9 0.1 copy.63
  29.0 0.1 eq.36
  29.1 0.1 fusion.29
  29.2 0.1 copy.64
  29.3 0.1 reduce_window_sum.11
  29.4 0.1 convolution_add_fusion.1
  29.5 0.0 copy-done.13
  29.6 0.1 convolution_add_fusion.2
  29.7 0.0 copy-done.11
  29.7 0.0 copy-start.9
  29.8 0.1 copy.56
  29.9 0.1 copy.57
  29.9 0.2 select_reduce_fusion
  30.2 61.5 %reduce-scatter.7.cloned.1.call-done = f32[32,1024]{1,0:T(8,128)} async-done(((f32[256,1024]{1,0:T(8,128)}), f32[32,1024]{1,0:T(8,128)}) %reduce-scatter.7.cloned.1.call-update) | async-done | bytes 131088
  91.6 1.1 copy.73
  92.8 0.1 copy.60
  92.9 0.1 copy.74
  93.0 0.1 copy.58
  93.1 0.1 copy.59
  93.2 0.8 multiply_reduce_fusion.2
  93.9 0.1 copy.62
  94.0 6.0 %multiply_reduce_fusion = (f32[32,2,128]{2,1,0:T(2,128)S(1)}, f32[32,2,128,128]{3,2,1,0:T(8,128)}) fusion(f32[32,2,128]{2,1,0:T(2,128)S(1)} %copy.74, f32[32,2,128]{2,1,0:T(2,128)S(1)} %copy.59, f32[32,2,128]{2,1,0:T(2,128)S(1)} %get-tuple-element.8, f32[32,2,128,128]{3,2,1,0:T(8,128)} %param.32, f32[32,2]{1,0:T(8,128)S(1)} %copy.56), kind=kLoop, calls=%fused_computation | loop fusion | flops 5234688 | bytes 8519936
  100.0 0.1 copy.71
  100.1 0.3 convolution_convert_fusion.2
  100.4 7.1 %all-gather = bf16[128,2048]{1,0:T(8,128)(2,1)S(1)} all-gather(bf16[32,2048]{1,0:T(8,128)(2,1)S(1)} %convolution_convert_fusion.2), channel_id=2, replica_groups=mesh['ep'=8,'tp'=4] {'tp'}, dimensions={0}, use_global_device_ids=true | all-gather | bytes 655360 | tf_op jit(solution)/shard_map/all_gather | solution.py:151
  107.6 0.1 reduce_sum.77
  107.7 0.2 fusion.19
  107.8 0.1 fusion.21
  107.9 0.1 broadcast_in_dim.6
  108.1 0.1 reshape.157
  108.2 0.3 convolution_convert_fusion.1
  108.5 0.0 copy-start.1
  108.5 0.1 broadcast_in_dim.8
  108.6 29.8 %all_to_all.41 = bf16[8,32,2048]{2,1,0:T(8,128)(2,1)S(1)} all-to-all(bf16[8,32,2048]{2,1,0:T(8,128)(2,1)S(1)} %bitcast.62), channel_id=1, replica_groups=mesh['ep'=8,'tp'=4] {'ep'}, dimensions={0} | all-to-all | bytes 2097152 | tf_op jit(solution)/shard_map/all_to_all | solution.py:158
  138.4 0.7 fusion.3
  139.2 3.8 %convolution_convert_fusion = bf16[256,2048]{1,0:T(8,128)(2,1)} fusion(bf16[1,384,2048]{2,1,0:T(8,128)(2,1)S(1)} %copy-done, bf16[256,2048]{1,0:T(8,128)(2,1)S(1)} %bitcast.61, bf16[1,2048,384]{2,1,0:T(8,128)(2,1)} %param.38, f32[256,384]{1,0:T(8,128)S(1)} %fusion.3), kind=kOutput, calls=%fused_computation.2 | convolution fusion | flops 806420480 | bytes 5636096 | tf_op jit(solution)/shard_map/dot_general | solution.py:162
  142.9 0.0 reduce-scatter.5.cloned.1.call-update
  143.0 23.3 %reduce-scatter.5.cloned.1.call-done = bf16[256,512]{1,0:T(8,128)(2,1)} async-done(((bf16[256,2048]{1,0:T(8,128)(2,1)}), bf16[256,512]{1,0:T(8,128)(2,1)}) %reduce-scatter.5.cloned.1.call-update) | async-done | bytes 262160 | tf_op jit(solution)/shard_map/reduce_scatter | solution.py:163
  166.3 5.5 %all-to-all-start.2 = ((bf16[8,32,512]{2,1,0:T(8,128)(2,1)}), bf16[8,32,512]{2,1,0:T(8,128)(2,1)S(1)}, u32[]{:S(2)}, u32[]{:S(2)}) async-start(bf16[8,32,512]{2,1,0:T(8,128)(2,1)} %bitcast.76), calls=%async_computation.3 | async-start | bytes 524288 | tf_op jit(solution)/shard_map/all_to_all | solution.py:166
  171.9 0.1 copy.66
  172.0 0.1 copy.65
  172.1 0.1 mul.171
  172.2 0.1 multiply_reduce_fusion.1
  172.3 8.2 %all-to-all-done.2 = bf16[8,32,512]{2,1,0:T(8,128)(2,1)S(1)} async-done(((bf16[8,32,512]{2,1,0:T(8,128)(2,1)}), bf16[8,32,512]{2,1,0:T(8,128)(2,1)S(1)}, u32[]{:S(2)}, u32[]{:S(2)}) %all-to-all-start.2) | async-done | bytes 262176 | tf_op jit(solution)/shard_map/all_to_all | solution.py:166
  180.6 0.9 fusion.13
  (37 shorter events, 0.3 us)
Async XLA Ops:
  7.2 132.0 %copy-start = (bf16[1,384,2048]{2,1,0:T(8,128)(2,1)S(1)}, bf16[1,384,2048]{2,1,0:T(8,128)(2,1)}, u32[]{:S(2)}) copy-start(bf16[1,384,2048]{2,1,0:T(8,128)(2,1)} %param.39) | copy-start | bytes 4718596
  7.2 19.7 %copy-start.4 = (bf16[256,256]{1,0:T(8,128)(2,1)S(1)}, bf16[256,256]{1,0:T(8,128)(2,1)}, u32[]{:S(2)}) copy-start(bf16[256,256]{1,0:T(8,128)(2,1)} %param.24) | copy-start | bytes 393220
  7.2 19.9 %copy-start.5 = (bf16[256,256]{1,0:T(8,128)(2,1)S(1)}, bf16[256,256]{1,0:T(8,128)(2,1)}, u32[]{:S(2)}) copy-start(bf16[256,256]{1,0:T(8,128)(2,1)} %param.23) | copy-start | bytes 393220
  7.2 84.4 %reduce-scatter.7.cloned.1.call-start = ((), (), s32[]{:S(2)}) async-start(), calls=%async_computation.6 | async-start | bytes 1179648
  27.4 1.5 copy-start.7
  27.4 1.5 copy-start.10
  27.5 1.9 %copy-start.12 = (bf16[2048,8]{0,1:T(8,128)(2,1)S(1)}, bf16[2048,8]{0,1:T(8,128)(2,1)}, u32[]{:S(2)}) copy-start(bf16[2048,8]{0,1:T(8,128)(2,1)} %param.27) | copy-start | bytes 98308
  27.5 1.9 %copy-start.14 = (f32[8]{0:T(128)S(1)}, f32[8]{0:T(128)}, u32[]{:S(2)}) copy-start(f32[8]{0:T(128)} %param.29) | copy-start | bytes 100
  27.5 2.1 %copy-start.13 = (bf16[2048,8]{0,1:T(8,128)(2,1)S(1)}, bf16[2048,8]{0,1:T(8,128)(2,1)}, u32[]{:S(2)}) copy-start(bf16[2048,8]{0,1:T(8,128)(2,1)} %param.28) | copy-start | bytes 98308
  27.5 2.1 %copy-start.15 = (f32[8]{0:T(128)S(1)}, f32[8]{0:T(128)}, u32[]{:S(2)}) copy-start(f32[8]{0:T(128)} %param.30) | copy-start | bytes 100
  27.5 2.2 %copy-start.11 = (f32[32,2]{0,1:T(2,128)S(1)}, f32[32,2]{0,1:T(2,128)}, u32[]{:S(2)}) copy-start(f32[32,2]{0,1:T(2,128)} %param.34) | copy-start | bytes 772
  28.8 64.3 %copy-start.6 = (f32[32,2,128]{2,1,0:T(2,128)S(1)}, f32[32,2,128]{2,1,0:T(2,128)}, u32[]{:S(2)}) copy-start(f32[32,2,128]{2,1,0:T(2,128)} %param.33) | copy-start | bytes 98308
  28.8 137.4 %reduce-scatter.5.cloned.1.call-start = ((), (), s32[]{:S(2)}) async-start(), calls=%async_computation.5 | async-start | bytes 1310720 | tf_op jit(solution)/shard_map/reduce_scatter | solution.py:163
  29.7 70.2 %copy-start.9 = (f32[32,2]{0,1:T(2,128)}, f32[32,2]{0,1:T(2,128)S(1)}, u32[]{:S(2)}) copy-start(f32[32,2]{0,1:T(2,128)S(1)} %get-tuple-element.12) | copy-start | bytes 772
  94.0 6.1 %copy-start.3 = (bf16[256,2048]{1,0:T(8,128)(2,1)S(1)}, bf16[256,2048]{1,0:T(8,128)(2,1)}, u32[]{:S(2)}) copy-start(bf16[256,2048]{1,0:T(8,128)(2,1)} %param.31) | copy-start | bytes 3145732
  100.0 7.7 %copy-start.2 = (bf16[32,2048]{1,0:T(8,128)(2,1)S(1)}, bf16[32,2048]{1,0:T(8,128)(2,1)}, u32[]{:S(2)}) copy-start(bf16[32,2048]{1,0:T(8,128)(2,1)} %param.20) | copy-start | bytes 393220
  108.5 29.9 %copy-start.1 = (bf16[1,2048,384]{2,1,0:T(8,128)(2,1)S(1)}, bf16[1,2048,384]{2,1,0:T(8,128)(2,1)}, u32[]{:S(2)}) copy-start(bf16[1,2048,384]{2,1,0:T(8,128)(2,1)} %param.37) | copy-start | bytes 4718596
  142.9 28.9 %copy-start.8 = (f32[32,2]{0,1:T(2,128)S(1)}, f32[32,2]{0,1:T(2,128)}, u32[]{:S(2)}) copy-start(f32[32,2]{0,1:T(2,128)} %param.36) | copy-start | bytes 772
  166.3 14.3 %all-to-all-start.2 = ((bf16[8,32,512]{2,1,0:T(8,128)(2,1)}), bf16[8,32,512]{2,1,0:T(8,128)(2,1)S(1)}, u32[]{:S(2)}, u32[]{:S(2)}) async-start(bf16[8,32,512]{2,1,0:T(8,128)(2,1)} %bitcast.76), calls=%async_computation.3 | async-start | bytes 524288 | tf_op jit(solution)/shard_map/all_to_all | solution.py:166
Sparse Core Ops, SparseCore 0:
  29.0 62.5 reduce-scatter.6
  143.1 23.1 reduce-scatter.4
